TPU v7x, 32 devices: a whole 2x2x4 slice. The times are simulated.
32 devices in a mesh: tp: 8 (over z, x), dp: 4 (over y, core).
Axes of the slice: x: 2, y: 2, z: 4, core: 2. Of those that a mesh axis runs over, the one named last changes fastest.
Arguments:
- tokens: bfloat16 [112, 4096], P('tp', 'dp'), may hold values from -6 to 6
- w_query: bfloat16 [2, 4096, 4096], P(None, 'dp', 'tp'), may hold values from -0.09375 to 0.09375
- w_key: bfloat16 [2, 4096, 4096], P(None, 'dp', 'tp'), may hold values from -0.09375 to 0.09375
- w_value: bfloat16 [2, 4096, 4096], P(None, 'dp', 'tp'), may hold values from -0.09375 to 0.09375
- w_outgate: bfloat16 [2, 4096, 4096], P(None, 'dp', 'tp'), may hold values from -0.09375 to 0.09375
- w_ingate: bfloat16 [2, 4096, 32], P(None, 'dp'), may hold values from -0.09375 to 0.09375
- w_forget: bfloat16 [2, 4096, 32], P(None, 'dp'), may hold values from -0.09375 to 0.09375
- forget_bias: float32 [2, 32], P(None, 'tp'), may hold values from -2 to 3
- head_gain: float32 [2, 32, 128], P(None, 'tp'), may hold values from 0.1 to 1.9
- w_proj: bfloat16 [2, 4096, 4096], P(None, 'tp', 'dp'), may hold values from -0.09375 to 0.09375
- mem_matrix: float32 [2, 112, 32, 128, 128], P(None, 'dp', 'tp'), may hold values from -0.8 to 0.8
- mem_norm: float32 [2, 112, 32, 128], P(None, 'dp', 'tp'), may hold values from -1.2 to 1.2
- mem_max: float32 [2, 112, 32], P(None, 'dp', 'tp'), may hold values from -4 to 4
Outputs:
- result: bfloat16 [112, 4096], P('tp', 'dp')
- new_matrix: float32 [2, 112, 32, 128, 128], P(None, 'dp', 'tp')
- new_norm: float32 [2, 112, 32, 128], P(None, 'dp', 'tp')
- new_max: float32 [2, 112, 32], P(None, 'dp', 'tp')
All inputs are finite; a program needn't handle non-finite values.
Results may differ from a plain program's by a relative error of at most 0.017.
Values may be sent and summed in bfloat16 or wider, within the bound.
A program may use at most 128 MiB of HBM per device.

v0:
```python
import jax
import jax.numpy as jnp
from jax import lax
from jax.sharding import PartitionSpec as P

HEAD = 128
norm_eps = 1e-06
head_eps = 1e-05


def cell_update(queries, key_vecs, values, log_in, log_forget, matrix, normvec, maxval):
    max_next = jnp.maximum(log_forget + maxval, log_in)
    decays = jnp.exp(log_forget + maxval - max_next)
    weight_in = jnp.exp(log_in - max_next)
    matrix_new = (
        decays[..., None, None] * matrix
        + weight_in[..., None, None] * key_vecs[..., :, None] * values[..., None, :]
    )
    norm_new = decays[..., None] * normvec + weight_in[..., None] * key_vecs
    numerator = jnp.einsum("bhd,bhde->bhe", queries, matrix_new, precision=lax.Precision.HIGHEST)
    denominator = jnp.maximum(jnp.abs(jnp.sum(queries * norm_new, axis=-1)), 1.0)
    return (numerator / denominator[..., None], matrix_new, norm_new, max_next)


def head_norm(readout, gain, outgate):
    average = jnp.mean(readout, axis=-1, keepdims=True)
    variance = jnp.mean(jnp.square(readout - average), axis=-1, keepdims=True)
    normed = (readout - average) * lax.rsqrt(variance + head_eps) * gain
    return normed * jax.nn.sigmoid(outgate)


def mix_block(gathered, weights, states):
    w_query, w_key, w_value, w_outgate, w_ingate, w_forget, bias, gain, w_proj = weights
    matrix, normvec, maxval = states
    features = gathered.shape[1] * lax.axis_size("dp")
    squares = jnp.sum(jnp.square(gathered.astype(jnp.float32)), axis=1)
    heads_dev = bias.shape[0]
    head_start = lax.axis_index("tp") * heads_dev
    gate_in = lax.dynamic_slice_in_dim(w_ingate, head_start, heads_dev, 1)
    gate_forget = lax.dynamic_slice_in_dim(w_forget, head_start, heads_dev, 1)
    part_query = jnp.dot(gathered, w_query, preferred_element_type=jnp.float32)
    part_key = jnp.dot(gathered, w_key, preferred_element_type=jnp.float32)
    part_value = jnp.dot(gathered, w_value, preferred_element_type=jnp.float32)
    part_outgate = jnp.dot(gathered, w_outgate, preferred_element_type=jnp.float32)
    part_ingate = jnp.dot(gathered, gate_in, preferred_element_type=jnp.float32)
    part_forget = jnp.dot(gathered, gate_forget, preferred_element_type=jnp.float32)
    rows_dev = gathered.shape[0] // lax.axis_size("dp")
    totals = lax.psum(squares, "dp")
    own_sum = lax.dynamic_slice_in_dim(totals, lax.axis_index("dp") * rows_dev, rows_dev, 0)
    sum_query, sum_key, sum_value, sum_outgate, sum_ingate, sum_forget = (
        lax.psum_scatter(part_query, "dp", scatter_dimension=0, tiled=True),
        lax.psum_scatter(part_key, "dp", scatter_dimension=0, tiled=True),
        lax.psum_scatter(part_value, "dp", scatter_dimension=0, tiled=True),
        lax.psum_scatter(part_outgate, "dp", scatter_dimension=0, tiled=True),
        lax.psum_scatter(part_ingate, "dp", scatter_dimension=0, tiled=True),
        lax.psum_scatter(part_forget, "dp", scatter_dimension=0, tiled=True),
    )
    inv_scale = lax.rsqrt(own_sum / features + norm_eps)[:, None]
    head_shape = (rows_dev, heads_dev, HEAD)
    queries = (sum_query * inv_scale).reshape(head_shape)
    key_vecs = (sum_key * inv_scale * HEAD ** (-0.5)).reshape(head_shape)
    values = (sum_value * inv_scale).reshape(head_shape)
    outgate = (sum_outgate * inv_scale).reshape(head_shape)
    log_in = sum_ingate * inv_scale
    log_forget = jax.nn.log_sigmoid(sum_forget * inv_scale + bias[None, :])
    readout, matrix_new, norm_new, max_next = cell_update(
        queries, key_vecs, values, log_in, log_forget, matrix, normvec, maxval
    )
    hidden = head_norm(readout, gain[None], outgate).reshape(rows_dev, -1).astype(jnp.bfloat16)
    out_partial = jnp.dot(
        lax.all_gather(hidden, "dp", axis=0, tiled=True), w_proj, preferred_element_type=jnp.float32
    )
    return (out_partial, matrix_new, norm_new, max_next)


def on_device(
    tokens,
    w_query,
    w_key,
    w_value,
    w_outgate,
    w_ingate,
    w_forget,
    forget_bias,
    head_gain,
    w_proj,
    mem_matrix,
    mem_norm,
    mem_max,
):
    current = lax.all_gather(tokens, "tp", axis=0, tiled=True)
    matrix_list, norm_list, max_list = ([], [], [])
    block_total = w_query.shape[0]
    result = current
    for block_id in range(block_total):
        weights = (
            w_query[block_id],
            w_key[block_id],
            w_value[block_id],
            w_outgate[block_id],
            w_ingate[block_id],
            w_forget[block_id],
            forget_bias[block_id],
            head_gain[block_id],
            w_proj[block_id],
        )
        out_partial, matrix_out, norm_out, max_out = mix_block(
            current, weights, (mem_matrix[block_id], mem_norm[block_id], mem_max[block_id])
        )
        matrix_list.append(matrix_out)
        norm_list.append(norm_out)
        max_list.append(max_out)
        if block_id + 1 < block_total:
            current = lax.psum(out_partial, "tp").astype(jnp.bfloat16)
        else:
            result = lax.psum_scatter(
                out_partial.astype(jnp.bfloat16), "tp", scatter_dimension=0, tiled=True
            )
    return (result, jnp.stack(matrix_list), jnp.stack(norm_list), jnp.stack(max_list))


def solution(mesh):
    in_specs = (
        P("tp", "dp"),
        P(None, "dp", "tp"),
        P(None, "dp", "tp"),
        P(None, "dp", "tp"),
        P(None, "dp", "tp"),
        P(None, "dp", None),
        P(None, "dp", None),
        P(None, "tp"),
        P(None, "tp", None),
        P(None, "tp", "dp"),
        P(None, "dp", "tp", None, None),
        P(None, "dp", "tp", None),
        P(None, "dp", "tp"),
    )
    out_specs = (
        P("tp", "dp"),
        P(None, "dp", "tp", None, None),
        P(None, "dp", "tp", None),
        P(None, "dp", "tp"),
    )
    return jax.shard_map(
        on_device, mesh=mesh, in_specs=in_specs, out_specs=out_specs, check_vma=False
    )
```

profile of v0, /device:TPU:0, one launch (start us, length us, event | category | flops | bytes accessed | tf_op | source)
XLA Modules:
  0.0 243.8 jit_solution(15858441146114237513)
XLA Ops:
  0.7 32.9 %all-gather = bf16[8,14,1024]{2,1,0:T(8,128)(2,1)S(1)} all-gather(bf16[1,14,1024]{2,1,0:T(8,128)(2,1)} %bitcast.149), channel_id=1, replica_groups=mesh['tp'=8,'dp'=4] {'tp'}, dimensions={0}, use_global_device_ids=true | all-gather | bytes 258048 | tf_op jit(solution)/shard_map/all_gather | solution.py:91
  33.6 1.5 fusion.36
  35.2 1.5 fusion.38
  36.7 1.5 fusion.40
  38.2 2.4 fusion.42
  40.6 14.0 %fusion.93 = (f32[32,512]{1,0:T(8,128)S(1)}, f32[32,512]{1,0:T(8,128)S(1)}, f32[32,512]{1,0:T(8,128)S(1)}, f32[32,512]{1,0:T(8,128)S(1)}) fusion(f32[112,512]{1,0:T(8,128)S(1)} %fusion.36, f32[112,512]{1,0:T(8,128)} %fusion.42, f32[112,512]{1,0:T(8,128)S(1)} %fusion.38, f32[112,512]{1,0:T(8,128)S(1)} %fusion.40), kind=kCustom, calls=%all-reduce-scatter.10 | all-reduce-scatter fusion | flops 262145 | bytes 1180160
  54.6 1.3 collective-permute-start.1
  55.9 3.7 %collective-permute-start.2 = (f32[12,512]{1,0:T(8,128)S(1)}, f32[12,512]{1,0:T(8,128)S(1)}, u32[]{:S(2)}, u32[]{:S(2)}) collective-permute-start(f32[12,512]{1,0:T(8,128)S(1)} %slice.98), channel_id=1, source_target_pairs={{0,1},{1,2},{2,3},{4,5},{5,6},{6,7},{8,9},{9,10},{10,11},{12,13},{... | collective-permute-start | bytes 73736
  59.6 1.9 collective-permute-start
  61.6 1.9 collective-permute-start.3
  63.5 0.1 multiply_reduce_fusion.1
  63.6 1.3 slice_bitcast_fusion.2
  64.9 0.9 fusion.99
  65.8 0.2 convolution_bitcast_fusion
  66.0 0.2 convolution_bitcast_fusion.1
  66.1 1.3 fusion.100
  68.1 5.8 %all-reduce.23 = (f32[112]{0:T(128)S(1)}, f32[112,4]{0,1:T(4,128)S(1)}, f32[112,4]{0,1:T(4,128)S(1)}) all-reduce(f32[112]{0:T(128)S(1)} %multiply_reduce_fusion.1, f32[112,4]{0,1:T(4,128)S(1)} %convolution_bitcast_fusion.1, f32[112,4]{0,1:T(4,128)S(1)} %convolution_bitcast_fusion), channel_id=1, replica_groups=mesh['tp'=8,'dp'=4] {'dp'}, use_global_device_ids=true, to_apply=%region_2.0 | all-reduce | flops 1008 | bytes 8064 | tf_op jit(solution)/shard_map/psum | solution.py:48
  74.1 0.8 maximum_bitcast_fusion.1
  74.9 0.7 slice_bitcast_fusion
  75.6 1.2 dynamic-slice.64
  78.4 0.2 concatenate.1
  78.6 0.2 concatenate.2
  78.8 0.2 concatenate
  79.0 0.2 concatenate.3
  79.4 0.2 fusion.69
  79.7 9.2 %fusion.13 = f32[28,4,1,128]{3,2,1,0:T(1,128)S(1)} fusion(f32[28,4,128,1]{2,3,1,0:T(1,128)S(1)} %bitcast.148, f32[2,28,4,128,128]{4,3,2,1,0:T(8,128)} %param.23, f32[28,4,128]{2,1,0:T(4,128)S(1)} %mul.321, f32[28,4,128]{2,1,0:T(4,128)S(1)} %get-tuple-element.37, f32[28,4]{1,0:T(8,128)S(1)} %copy.41), kind=kOutput, calls=%fused_computation.6 | convolution fusion | flops 27525120 | bytes 7569856 | tf_op jit(solution)/shard_map/bhd,bhde->bhe/dot_general | solution.py:20
  88.9 0.2 fusion.97
  89.1 0.2 multiply_reduce_fusion.3
  89.3 0.1 multiply_convert_fusion.1
  89.4 5.4 %all-gather.1 = bf16[4,28,512]{2,1,0:T(8,128)(2,1)S(1)} all-gather(bf16[1,28,512]{2,1,0:T(8,128)(2,1)S(1)} %reshape.136), channel_id=1, replica_groups=mesh['tp'=8,'dp'=4] {'dp'}, dimensions={0}, use_global_device_ids=true | all-gather | bytes 143360 | tf_op jit(solution)/shard_map/all_gather | solution.py:71
  94.9 0.3 fusion.34
  95.2 43.0 %all-reduce.27 = bf16[112,1024]{1,0:T(8,128)(2,1)S(1)} all-reduce(f32[112,1024]{1,0:T(8,128)S(1)} %fusion.34), channel_id=1, replica_groups=mesh['tp'=8,'dp'=4] {'tp'}, use_global_device_ids=true, to_apply=%region_11.12 | all-reduce | flops 114688 | bytes 688128 | tf_op jit(solution)/shard_map/psum | solution.py:114
  138.2 0.1 multiply_reduce_fusion
  138.4 1.5 fusion.28
  139.9 1.5 fusion.30
  141.4 1.5 fusion.32
  143.0 1.5 fusion.26
  144.5 0.2 fusion.70
  144.7 0.2 fusion.72
  144.8 5.7 %all-reduce.22 = (f32[112]{0:T(128)S(1)}, f32[112,4]{0,1:T(4,128)S(1)}, f32[112,4]{0,1:T(4,128)S(1)}) all-reduce(f32[112]{0:T(128)S(1)} %multiply_reduce_fusion, f32[112,4]{0,1:T(4,128)S(1)} %fusion.72, f32[112,4]{0,1:T(4,128)S(1)} %fusion.70), channel_id=1, replica_groups=mesh['tp'=8,'dp'=4] {'dp'}, use_global_device_ids=true, to_apply=%region_14.15 | all-reduce | flops 1008 | bytes 8064 | tf_op jit(solution)/shard_map/psum | solution.py:48
  150.9 14.6 %fusion.92 = (f32[32,512]{1,0:T(8,128)S(1)}, f32[32,512]{1,0:T(8,128)S(1)}, f32[32,512]{1,0:T(8,128)S(1)}, f32[32,512]{1,0:T(8,128)S(1)}) fusion(f32[112,512]{1,0:T(8,128)S(1)} %fusion.26, f32[112,512]{1,0:T(8,128)S(1)} %fusion.32, f32[112,512]{1,0:T(8,128)S(1)} %fusion.28, f32[112,512]{1,0:T(8,128)S(1)} %fusion.30), kind=kCustom, calls=%all-reduce-scatter.9 | all-reduce-scatter fusion | flops 262145 | bytes 1180160
  165.5 1.3 collective-permute-start.5
  166.8 3.8 %collective-permute-start.6 = (f32[12,512]{1,0:T(8,128)S(1)}, f32[12,512]{1,0:T(8,128)S(1)}, u32[]{:S(2)}, u32[]{:S(2)}) collective-permute-start(f32[12,512]{1,0:T(8,128)S(1)} %slice.102), channel_id=1, source_target_pairs={{0,1},{1,2},{2,3},{4,5},{5,6},{6,7},{8,9},{9,10},{10,11},{12,13},{... | collective-permute-start | bytes 73736
  170.6 1.9 collective-permute-start.4
  172.6 2.1 collective-permute-start.7
  174.7 0.6 pad_maximum_fusion.2
  175.5 0.2 concatenate.5
  175.7 0.2 concatenate.6
  175.9 0.2 concatenate.4
  176.1 0.2 concatenate.7
  176.6 0.2 fusion.66
  176.8 14.1 %multiply_add_fusion.1 = (f32[1,28,4,128,128]{4,3,2,1,0:T(8,128)}, f32[1,28,4,128,128]{4,3,2,1,0:T(8,128)}) fusion(f32[2,28,4,128,128]{4,3,2,1,0:T(8,128)} %param.23, f32[28,4,128]{2,1,0:T(4,128)S(1)} %mul.321, f32[28,4,128]{2,1,0:T(4,128)S(1)} %get-tuple-element.37, f32[28,4]{1,0:T(8,128)S(1)} %copy.41, f32[28,4,128]{2,1,0:T(4,128)S(1)} %mul.347, ...), kind=kLoop, calls=%fused_computation.8 | loop fusion | flops 11010048 | bytes 29590400 | tf_op jit(solution)/shard_map/add | solution.py:16
  190.9 6.9 %fusion.10 = f32[28,4,1,128]{3,2,1,0:T(1,128)S(1)} fusion(f32[28,4,128,1]{2,3,1,0:T(1,128)S(1)} %bitcast.147, f32[2,28,4,128,128]{4,3,2,1,0:T(8,128)S(1)} %bitcast.144, f32[28,4,128]{2,1,0:T(4,128)S(1)} %mul.347, f32[28,4,128]{2,1,0:T(4,128)S(1)} %get-tuple-element.33, f32[28,4]{1,0:T(8,128)S(1)} %copy.44), kind=kOutput, calls=%fused_computation.3 | convolution fusion | flops 27525120 | bytes 7585792 | tf_op jit(solution)/shard_map/bhd,bhde->bhe/dot_general | solution.py:20
  197.9 0.2 fusion.96
  198.1 0.2 multiply_reduce_fusion.2
  198.4 5.4 %all-gather.2 = bf16[4,28,512]{2,1,0:T(8,128)(2,1)S(1)} all-gather(bf16[1,28,512]{2,1,0:T(8,128)(2,1)S(1)} %reshape.138), channel_id=1, replica_groups=mesh['tp'=8,'dp'=4] {'dp'}, dimensions={0}, use_global_device_ids=true | all-gather | bytes 143360 | tf_op jit(solution)/shard_map/all_gather | solution.py:71
  203.9 1.5 convolution_convert_fusion
  205.4 21.2 %fusion.8 = bf16[16,1024]{1,0:T(8,128)(2,1)S(1)} fusion(bf16[112,1024]{1,0:T(8,128)(2,1)S(1)} %convolution_convert_fusion), kind=kCustom, calls=%all-reduce-scatter.8 | all-reduce-scatter fusion | flops 131073 | bytes 262656
  226.6 2.1 collective-permute-start.8
  228.7 0.2 multiply_add_fusion.3
  228.9 13.4 %pad_maximum_fusion = f32[2,28,4,128,128]{4,3,2,1,0:T(8,128)} fusion(f32[1,28,4,128,128]{4,3,2,1,0:T(8,128)} %get-tuple-element.39, f32[1,28,4,128,128]{4,3,2,1,0:T(8,128)} %get-tuple-element.38), kind=kLoop, calls=%fused_computation | loop fusion | flops 3670016 | bytes 29360128 | tf_op jit(solution)/shard_map/stack | solution.py:119
  242.3 0.7 pad_maximum_fusion.1
  242.9 0.2 concatenate.8
  243.1 0.6 constant_dynamic-slice_fusion
  (73 shorter events, 1.8 us)
Async XLA Ops:
  0.6 64.3 %copy-start.2 = (bf16[2,1024,32]{1,2,0:T(8,128)(2,1)S(1)}, bf16[2,1024,32]{1,2,0:T(8,128)(2,1)}, u32[]{:S(2)}) copy-start(bf16[2,1024,32]{1,2,0:T(8,128)(2,1)} %param.18) | copy-start | bytes 393220
  0.6 78.8 %copy-start.1 = (f32[2,28,4,128]{3,2,1,0:T(4,128)S(1)}, f32[2,28,4,128]{3,2,1,0:T(4,128)}, u32[]{:S(2)}) copy-start(f32[2,28,4,128]{3,2,1,0:T(4,128)} %param.24) | copy-start | bytes 344068
  38.2 56.7 %copy-start = (bf16[2,512,1024]{2,1,0:T(8,128)(2,1)S(1)}, bf16[2,512,1024]{2,1,0:T(8,128)(2,1)}, u32[]{:S(2)}) copy-start(bf16[2,512,1024]{2,1,0:T(8,128)(2,1)} %param.22) | copy-start | bytes 6291460
  54.6 23.8 %collective-permute-start.1 = (f32[12,512]{1,0:T(8,128)S(1)}, f32[12,512]{1,0:T(8,128)S(1)}, u32[]{:S(2)}, u32[]{:S(2)}) collective-permute-start(f32[12,512]{1,0:T(8,128)S(1)} %slice.97), channel_id=1, source_target_pairs={{0,1},{1,2},{2,3},{4,5},{5,6},{6,7},{8,9},{9,10},{10,11},{12,13},{... | collective-permute-start | bytes 73736
  55.9 22.6 %collective-permute-start.2 = (f32[12,512]{1,0:T(8,128)S(1)}, f32[12,512]{1,0:T(8,128)S(1)}, u32[]{:S(2)}, u32[]{:S(2)}) collective-permute-start(f32[12,512]{1,0:T(8,128)S(1)} %slice.98), channel_id=1, source_target_pairs={{0,1},{1,2},{2,3},{4,5},{5,6},{6,7},{8,9},{9,10},{10,11},{12,13},{... | collective-permute-start | bytes 73736
  59.6 19.2 %collective-permute-start = (f32[12,512]{1,0:T(8,128)S(1)}, f32[12,512]{1,0:T(8,128)S(1)}, u32[]{:S(2)}, u32[]{:S(2)}) collective-permute-start(f32[12,512]{1,0:T(8,128)S(1)} %slice.96), channel_id=1, source_target_pairs={{0,1},{1,2},{2,3},{4,5},{5,6},{6,7},{8,9},{9,10},{10,11},{12,13},{... | collective-permute-start | bytes 73736
  61.6 17.4 %collective-permute-start.3 = (f32[12,512]{1,0:T(8,128)S(1)}, f32[12,512]{1,0:T(8,128)S(1)}, u32[]{:S(2)}, u32[]{:S(2)}) collective-permute-start(f32[12,512]{1,0:T(8,128)S(1)} %slice.99), channel_id=1, source_target_pairs={{0,1},{1,2},{2,3},{4,5},{5,6},{6,7},{8,9},{9,10},{10,11},{12,13},{... | collective-permute-start | bytes 73736
  79.7 71.0 %copy-start.3 = (f32[2,28,4]{1,2,0:T(4,128)S(1)}, f32[2,28,4]{1,2,0:T(4,128)}, u32[]{:S(2)}) copy-start(f32[2,28,4]{1,2,0:T(4,128)} %param.25) | copy-start | bytes 2692
  79.7 71.0 %copy-start.4 = (f32[4]{0:T(128)S(1)}, f32[4]{0:T(128)}, u32[]{:S(2)}) copy-start(f32[4]{0:T(128)} %get-tuple-element.52) | copy-start | bytes 52
  165.5 10.0 %collective-permute-start.5 = (f32[12,512]{1,0:T(8,128)S(1)}, f32[12,512]{1,0:T(8,128)S(1)}, u32[]{:S(2)}, u32[]{:S(2)}) collective-permute-start(f32[12,512]{1,0:T(8,128)S(1)} %slice.101), channel_id=1, source_target_pairs={{0,1},{1,2},{2,3},{4,5},{5,6},{6,7},{8,9},{9,10},{10,11},{12,13},{... | collective-permute-start | bytes 73736
  166.8 8.9 %collective-permute-start.6 = (f32[12,512]{1,0:T(8,128)S(1)}, f32[12,512]{1,0:T(8,128)S(1)}, u32[]{:S(2)}, u32[]{:S(2)}) collective-permute-start(f32[12,512]{1,0:T(8,128)S(1)} %slice.102), channel_id=1, source_target_pairs={{0,1},{1,2},{2,3},{4,5},{5,6},{6,7},{8,9},{9,10},{10,11},{12,13},{... | collective-permute-start | bytes 73736
  170.6 5.2 %collective-permute-start.4 = (f32[12,512]{1,0:T(8,128)S(1)}, f32[12,512]{1,0:T(8,128)S(1)}, u32[]{:S(2)}, u32[]{:S(2)}) collective-permute-start(f32[12,512]{1,0:T(8,128)S(1)} %slice.100), channel_id=1, source_target_pairs={{0,1},{1,2},{2,3},{4,5},{5,6},{6,7},{8,9},{9,10},{10,11},{12,13},{... | collective-permute-start | bytes 73736
  172.6 3.5 %collective-permute-start.7 = (f32[12,512]{1,0:T(8,128)S(1)}, f32[12,512]{1,0:T(8,128)S(1)}, u32[]{:S(2)}, u32[]{:S(2)}) collective-permute-start(f32[12,512]{1,0:T(8,128)S(1)} %slice.103), channel_id=1, source_target_pairs={{0,1},{1,2},{2,3},{4,5},{5,6},{6,7},{8,9},{9,10},{10,11},{12,13},{... | collective-permute-start | bytes 73736
  176.5 14.4 %slice-start = ((s8[14680064]{0:T(1024)(128)(4,1)}), s8[2097152]{0:T(1024)(128)(4,1)S(1)}, s32[]{:S(2)}) async-start(s8[14680064]{0:T(1024)(128)(4,1)} %bitcast.143), calls=%async_computation | async-start | bytes 4194304
  176.8 14.1 %slice-start.1 = ((s8[14680064]{0:T(1024)(128)(4,1)}), s8[4194304]{0:T(1024)(128)(4,1)S(1)}, s32[]{:S(2)}) async-start(s8[14680064]{0:T(1024)(128)(4,1)} %bitcast.143), calls=%async_computation.1 | async-start | bytes 8388608
  176.8 14.1 %slice-start.2 = ((s8[14680064]{0:T(1024)(128)(4,1)}), s8[4194304]{0:T(1024)(128)(4,1)S(1)}, s32[]{:S(2)}) async-start(s8[14680064]{0:T(1024)(128)(4,1)} %bitcast.143), calls=%async_computation.2 | async-start | bytes 8388608
  176.8 14.1 %slice-start.3 = ((s8[14680064]{0:T(1024)(128)(4,1)}), s8[4194304]{0:T(1024)(128)(4,1)S(1)}, s32[]{:S(2)}) async-start(s8[14680064]{0:T(1024)(128)(4,1)} %bitcast.143), calls=%async_computation.3 | async-start | bytes 8388608
  226.6 16.3 %collective-permute-start.8 = (bf16[14,1024]{1,0:T(8,128)(2,1)S(1)}, bf16[14,1024]{1,0:T(8,128)(2,1)S(1)}, u32[]{:S(2)}, u32[]{:S(2)}) collective-permute-start(bf16[14,1024]{1,0:T(8,128)(2,1)S(1)} %slice.104), channel_id=1, source_target_pairs={{0,4},{4,8},{8,12},{12,16},{16,20},{20,24},{24,28},{1,5},{5,9},{9,... | collective-permute-start | bytes 86024
where the time goes:
time: 245 us; the launch traced here: 244 us
  blocking collectives  148 us (60%)
  other arithmetic  31.9 us (13%)
  matrix products  31.7 us (13%)
  starting transfers between devices  20 us (8%)
  local copies, waits for them, and re-layouts  8.64 us (4%)
  between operations  3.34 us (1%)
    unnamed x3, blocking collectives  49.8 us
    psum x1, blocking collectives, on_device(): current = lax.psum(out_partial, 'tp').astype(jnp.bfloat16)  43 us
    all_gather x1, blocking collectives, on_device(): current = lax.all_gather(tokens, 'tp', axis=0, tiled=True)  32.9 us
    unnamed x9, starting transfers between devices  20 us
    dot_general x2, matrix products, cell_update(): jnp.einsum('bhd,bhde->bhe', queries, matrix_new, precision=lax.Precision....  16.1 us
    add x1, other arithmetic, cell_update(): decays[..., None, None] * matrix  14.1 us
    another operation x1, other arithmetic, on_device(): jnp.stack(matrix_list)  13.4 us
    psum x2, blocking collectives, mix_block(): totals = lax.psum(squares, 'dp')  11.6 us
  transfers between devices with their start and end apart: 9, of which 0 were waited for; matrix products, arithmetic and copies ran while one was open for 10% of the time, Pallas kernels for 0%

commit v1 on v0

--- a/solution.py
+++ b/solution.py
@@ -111,7 +111,8 @@
         norm_list.append(norm_out)
         max_list.append(max_out)
         if block_id + 1 < block_total:
-            current = lax.psum(out_partial, "tp").astype(jnp.bfloat16)
+            touch_row = lambda sheet, axis_key: jnp.sum(jax.lax.all_gather(sheet, axis_key), 0)
+            current = touch_row(out_partial, "tp").astype(jnp.bfloat16)
         else:
             result = lax.psum_scatter(
                 out_partial.astype(jnp.bfloat16), "tp", scatter_dimension=0, tiled=True

time: 245 us -> 283 us (1.16)
  waiting for transfers between devices: 0.02 us -> 66.2 us
  blocking collectives: 148 us -> 107 us
  between operations: 3.34 us -> 16.8 us
    all_gather x0 -> x1, waiting for transfers between devices: none -> 66.2 us  [on_device(): jax.lax.all_gather(sheet, axis_key)]
    psum x1 -> x0, blocking collectives: 43 us -> none  [on_device(): current = lax.psum(out_partial, 'tp').astype(jnp.bfloat16)]
  transfers between devices with their start and end apart: 9 -> 10, of which waited for: 0 -> 1; matrix products, arithmetic and copies ran while one was open for 10% -> 7% of each run, Pallas kernels for 0% -> 0%
where the time goes in v1:
time: 283 us; the launch traced here: 282 us
  blocking collectives  107 us (38%)
  waiting for transfers between devices  66.2 us (23%)
  other arithmetic  33.7 us (12%)
  matrix products  32.4 us (11%)
  starting transfers between devices  19.5 us (7%)
  between operations  16.8 us (6%)
  local copies, waits for them, and re-layouts  6.18 us (2%)
    all_gather x1, waiting for transfers between devices, on_device(): jax.lax.all_gather(sheet, axis_key)  66.2 us
    unnamed x3, blocking collectives  51.8 us
    all_gather x1, blocking collectives, on_device(): current = lax.all_gather(tokens, 'tp', axis=0, tiled=True)  32.9 us
    unnamed x9, starting transfers between devices  19.4 us
    dot_general x2, matrix products, cell_update(): jnp.einsum('bhd,bhde->bhe', queries, matrix_new, precision=lax.Precision....  16.1 us
    add x1, other arithmetic, cell_update(): decays[..., None, None] * matrix  14.1 us
    another operation x1, other arithmetic, on_device(): jnp.stack(matrix_list)  13.4 us
    psum x2, blocking collectives, mix_block(): totals = lax.psum(squares, 'dp')  11.6 us
  transfers between devices with their start and end apart: 10, of which 1 were waited for; matrix products, arithmetic and copies ran while one was open for 7% of the time, Pallas kernels for 0%

profile of v1, /device:TPU:0, one launch (start us, length us, event | category | flops | bytes accessed | tf_op | source)
XLA Modules:
  0.0 281.9 jit_solution(1711170090528397764)
XLA Ops:
  7.3 32.9 %all-gather.1 = bf16[8,14,1024]{2,1,0:T(8,128)(2,1)S(1)} all-gather(bf16[1,14,1024]{2,1,0:T(8,128)(2,1)} %bitcast.151), channel_id=1, replica_groups=mesh['tp'=8,'dp'=4] {'tp'}, dimensions={0}, use_global_device_ids=true | all-gather | bytes 258048 | tf_op jit(solution)/shard_map/all_gather | solution.py:91
  40.2 1.5 fusion.36
  41.8 1.5 fusion.38
  43.3 1.5 fusion.40
  44.9 2.4 fusion.42
  47.2 14.0 %fusion.93 = (f32[32,512]{1,0:T(8,128)S(1)}, f32[32,512]{1,0:T(8,128)S(1)}, f32[32,512]{1,0:T(8,128)S(1)}, f32[32,512]{1,0:T(8,128)S(1)}) fusion(f32[112,512]{1,0:T(8,128)S(1)} %fusion.36, f32[112,512]{1,0:T(8,128)} %fusion.42, f32[112,512]{1,0:T(8,128)S(1)} %fusion.38, f32[112,512]{1,0:T(8,128)S(1)} %fusion.40), kind=kCustom, calls=%all-reduce-scatter.10 | all-reduce-scatter fusion | flops 262145 | bytes 1180160
  61.2 1.3 collective-permute-start.1
  62.6 3.7 %collective-permute-start.2 = (f32[12,512]{1,0:T(8,128)S(1)}, f32[12,512]{1,0:T(8,128)S(1)}, u32[]{:S(2)}, u32[]{:S(2)}) collective-permute-start(f32[12,512]{1,0:T(8,128)S(1)} %slice.98), channel_id=1, source_target_pairs={{0,1},{1,2},{2,3},{4,5},{5,6},{6,7},{8,9},{9,10},{10,11},{12,13},{... | collective-permute-start | bytes 73736
  66.3 1.9 collective-permute-start
  68.2 1.9 collective-permute-start.3
  70.1 0.1 multiply_reduce_fusion.1
  70.3 0.9 fusion.98
  71.2 0.9 fusion.99
  72.1 0.2 convolution_bitcast_fusion
  72.2 0.2 convolution_bitcast_fusion.1
  72.4 0.6 fusion.100
  73.7 5.8 %all-reduce.23 = (f32[112]{0:T(128)S(1)}, f32[112,4]{0,1:T(4,128)S(1)}, f32[112,4]{0,1:T(4,128)S(1)}) all-reduce(f32[112]{0:T(128)S(1)} %multiply_reduce_fusion.1, f32[112,4]{0,1:T(4,128)S(1)} %convolution_bitcast_fusion.1, f32[112,4]{0,1:T(4,128)S(1)} %convolution_bitcast_fusion), channel_id=1, replica_groups=mesh['tp'=8,'dp'=4] {'dp'}, use_global_device_ids=true, to_apply=%region_2.0 | all-reduce | flops 1008 | bytes 8064 | tf_op jit(solution)/shard_map/psum | solution.py:48
  80.7 0.2 concatenate.1
  80.9 0.2 concatenate.2
  81.1 0.2 concatenate
  81.3 0.2 concatenate.3
  81.7 0.2 fusion.69
  81.9 9.2 %fusion.13 = f32[28,4,1,128]{3,2,1,0:T(1,128)S(1)} fusion(f32[28,4,128,1]{2,3,1,0:T(1,128)S(1)} %bitcast.150, f32[2,28,4,128,128]{4,3,2,1,0:T(8,128)} %param.23, f32[28,4,128]{2,1,0:T(4,128)S(1)} %mul.321, f32[28,4,128]{2,1,0:T(4,128)S(1)} %get-tuple-element.37, f32[28,4]{1,0:T(8,128)S(1)} %copy.53), kind=kOutput, calls=%fused_computation.6 | convolution fusion | flops 27525120 | bytes 7569856 | tf_op jit(solution)/shard_map/bhd,bhde->bhe/dot_general | solution.py:20
  91.1 0.2 fusion.97
  91.3 0.2 multiply_reduce_fusion.3
  91.5 0.1 multiply_convert_fusion.1
  91.7 5.4 %all-gather.2 = bf16[4,28,512]{2,1,0:T(8,128)(2,1)S(1)} all-gather(bf16[1,28,512]{2,1,0:T(8,128)(2,1)S(1)} %reshape.137), channel_id=1, replica_groups=mesh['tp'=8,'dp'=4] {'dp'}, dimensions={0}, use_global_device_ids=true | all-gather | bytes 143360 | tf_op jit(solution)/shard_map/all_gather | solution.py:71
  97.1 1.1 fusion.34
  98.2 0.6 dynamic-slice.64
  99.5 66.2 %all-gather.6.cloned.1.call-done = f32[896,1024]{1,0:T(8,128)} async-done(((f32[112,1024]{1,0:T(8,128)}), f32[896,1024]{1,0:T(8,128)}) %all-gather.6.cloned.1.call-update) | async-done | bytes 3670032 | tf_op jit(solution)/shard_map/all_gather | solution.py:114
  165.7 2.4 reduce_sum.85
  168.1 0.1 multiply_reduce_fusion
  168.2 1.5 fusion.28
  169.7 1.5 fusion.30
  171.3 1.5 fusion.32
  172.8 1.5 fusion.26
  174.3 0.2 fusion.70
  174.5 0.2 fusion.72
  174.7 5.7 %all-reduce.22 = (f32[112]{0:T(128)S(1)}, f32[112,4]{0,1:T(4,128)S(1)}, f32[112,4]{0,1:T(4,128)S(1)}) all-reduce(f32[112]{0:T(128)S(1)} %multiply_reduce_fusion, f32[112,4]{0,1:T(4,128)S(1)} %fusion.72, f32[112,4]{0,1:T(4,128)S(1)} %fusion.70), channel_id=1, replica_groups=mesh['tp'=8,'dp'=4] {'dp'}, use_global_device_ids=true, to_apply=%region_14.15 | all-reduce | flops 1008 | bytes 8064 | tf_op jit(solution)/shard_map/psum | solution.py:48
  180.7 14.2 %fusion.92 = (f32[32,512]{1,0:T(8,128)S(1)}, f32[32,512]{1,0:T(8,128)S(1)}, f32[32,512]{1,0:T(8,128)S(1)}, f32[32,512]{1,0:T(8,128)S(1)}) fusion(f32[112,512]{1,0:T(8,128)S(1)} %fusion.26, f32[112,512]{1,0:T(8,128)S(1)} %fusion.32, f32[112,512]{1,0:T(8,128)S(1)} %fusion.28, f32[112,512]{1,0:T(8,128)S(1)} %fusion.30), kind=kCustom, calls=%all-reduce-scatter.9 | all-reduce-scatter fusion | flops 262145 | bytes 1180160
  195.0 1.3 collective-permute-start.5
  196.3 4.0 %collective-permute-start.6 = (f32[12,512]{1,0:T(8,128)S(1)}, f32[12,512]{1,0:T(8,128)S(1)}, u32[]{:S(2)}, u32[]{:S(2)}) collective-permute-start(f32[12,512]{1,0:T(8,128)S(1)} %slice.102), channel_id=1, source_target_pairs={{0,1},{1,2},{2,3},{4,5},{5,6},{6,7},{8,9},{9,10},{10,11},{12,13},{... | collective-permute-start | bytes 73736
  200.3 1.9 collective-permute-start.4
  202.2 2.1 collective-permute-start.7
  204.3 0.6 pad_maximum_fusion.2
  205.1 0.2 concatenate.5
  205.3 0.2 concatenate.6
  205.5 0.2 concatenate.4
  205.7 0.2 concatenate.7
  206.2 0.2 fusion.66
  206.5 14.1 %multiply_add_fusion.1 = (f32[1,28,4,128,128]{4,3,2,1,0:T(8,128)}, f32[1,28,4,128,128]{4,3,2,1,0:T(8,128)}) fusion(f32[2,28,4,128,128]{4,3,2,1,0:T(8,128)} %param.23, f32[28,4,128]{2,1,0:T(4,128)S(1)} %mul.321, f32[28,4,128]{2,1,0:T(4,128)S(1)} %get-tuple-element.37, f32[28,4]{1,0:T(8,128)S(1)} %copy.53, f32[28,4,128]{2,1,0:T(4,128)S(1)} %mul.347, ...), kind=kLoop, calls=%fused_computation.8 | loop fusion | flops 11010048 | bytes 29590400 | tf_op jit(solution)/shard_map/add | solution.py:16
  220.7 6.9 %fusion.10 = f32[28,4,1,128]{3,2,1,0:T(1,128)S(1)} fusion(f32[28,4,128,1]{2,3,1,0:T(1,128)S(1)} %bitcast.149, f32[2,28,4,128,128]{4,3,2,1,0:T(8,128)S(1)} %bitcast.145, f32[28,4,128]{2,1,0:T(4,128)S(1)} %mul.347, f32[28,4,128]{2,1,0:T(4,128)S(1)} %get-tuple-element.33, f32[28,4]{1,0:T(8,128)S(1)} %copy.56), kind=kOutput, calls=%fused_computation.3 | convolution fusion | flops 27525120 | bytes 7585792 | tf_op jit(solution)/shard_map/bhd,bhde->bhe/dot_general | solution.py:20
  227.6 0.2 fusion.96
  227.8 0.2 multiply_reduce_fusion.2
  228.0 0.1 multiply_convert_fusion
  228.1 5.4 %all-gather.3 = bf16[4,28,512]{2,1,0:T(8,128)(2,1)S(1)} all-gather(bf16[1,28,512]{2,1,0:T(8,128)(2,1)S(1)} %reshape.139), channel_id=1, replica_groups=mesh['tp'=8,'dp'=4] {'dp'}, dimensions={0}, use_global_device_ids=true | all-gather | bytes 143360 | tf_op jit(solution)/shard_map/all_gather | solution.py:71
  233.6 1.5 convolution_convert_fusion
  235.1 23.6 %fusion.8 = bf16[16,1024]{1,0:T(8,128)(2,1)S(1)} fusion(bf16[112,1024]{1,0:T(8,128)(2,1)S(1)} %convolution_convert_fusion), kind=kCustom, calls=%all-reduce-scatter.8 | all-reduce-scatter fusion | flops 131073 | bytes 262656
  258.7 1.3 collective-permute-start.8
  260.0 0.2 multiply_add_fusion.3
  260.2 13.4 %pad_maximum_fusion = f32[2,28,4,128,128]{4,3,2,1,0:T(8,128)} fusion(f32[1,28,4,128,128]{4,3,2,1,0:T(8,128)} %get-tuple-element.39, f32[1,28,4,128,128]{4,3,2,1,0:T(8,128)} %get-tuple-element.38), kind=kLoop, calls=%fused_computation | loop fusion | flops 3670016 | bytes 29360128 | tf_op jit(solution)/shard_map/stack | solution.py:120
  273.6 0.7 pad_maximum_fusion.1
  274.3 0.2 concatenate.8
  274.4 0.6 constant_dynamic-slice_fusion
  (80 shorter events, 1.8 us)
Async XLA Ops:
  7.2 65.2 %copy-start.4 = (u32[32]{0:T(128)S(1)}, u32[32]{0:T(128)}, u32[]{:S(2)}) copy-start(u32[32]{0:T(128)} %constant.56) | copy-start | bytes 388
  7.2 63.1 %copy-start.5 = (f32[2,4]{1,0:T(2,128)S(1)}, f32[2,4]{1,0:T(2,128)}, u32[]{:S(2)}) copy-start(f32[2,4]{1,0:T(2,128)} %param.20) | copy-start | bytes 100
  7.2 72.4 %copy-start.3 = (f32[2,28,4]{1,2,0:T(4,128)S(1)}, f32[2,28,4]{1,2,0:T(4,128)}, u32[]{:S(2)}) copy-start(f32[2,28,4]{1,2,0:T(4,128)} %param.25) | copy-start | bytes 2692
  7.2 72.6 %copy-start.2 = (f32[2,4,128]{2,1,0:T(4,128)S(1)}, f32[2,4,128]{2,1,0:T(4,128)}, u32[]{:S(2)}) copy-start(f32[2,4,128]{2,1,0:T(4,128)} %param.21) | copy-start | bytes 12292
  7.2 74.5 %copy-start.1 = (f32[2,28,4,128]{3,2,1,0:T(4,128)S(1)}, f32[2,28,4,128]{3,2,1,0:T(4,128)}, u32[]{:S(2)}) copy-start(f32[2,28,4,128]{3,2,1,0:T(4,128)} %param.24) | copy-start | bytes 344068
  7.2 158.5 %all-gather.6.cloned.1.call-start = ((), (), s32[]{:S(2)}) async-start(), calls=%async_computation | async-start | bytes 4128768 | tf_op jit(solution)/shard_map/all_gather | solution.py:114
  44.8 52.3 %copy-start = (bf16[2,512,1024]{2,1,0:T(8,128)(2,1)S(1)}, bf16[2,512,1024]{2,1,0:T(8,128)(2,1)}, u32[]{:S(2)}) copy-start(bf16[2,512,1024]{2,1,0:T(8,128)(2,1)} %param.22) | copy-start | bytes 6291460
  61.2 37.0 %copy-start.6 = (u32[32]{0:T(128)S(1)}, u32[32]{0:T(128)}, u32[]{:S(2)}) copy-start(u32[32]{0:T(128)} %constant.104) | copy-start | bytes 388
  61.2 19.4 %collective-permute-start.1 = (f32[12,512]{1,0:T(8,128)S(1)}, f32[12,512]{1,0:T(8,128)S(1)}, u32[]{:S(2)}, u32[]{:S(2)}) collective-permute-start(f32[12,512]{1,0:T(8,128)S(1)} %slice.97), channel_id=1, source_target_pairs={{0,1},{1,2},{2,3},{4,5},{5,6},{6,7},{8,9},{9,10},{10,11},{12,13},{... | collective-permute-start | bytes 73736
  62.6 18.3 %collective-permute-start.2 = (f32[12,512]{1,0:T(8,128)S(1)}, f32[12,512]{1,0:T(8,128)S(1)}, u32[]{:S(2)}, u32[]{:S(2)}) collective-permute-start(f32[12,512]{1,0:T(8,128)S(1)} %slice.98), channel_id=1, source_target_pairs={{0,1},{1,2},{2,3},{4,5},{5,6},{6,7},{8,9},{9,10},{10,11},{12,13},{... | collective-permute-start | bytes 73736
  66.3 14.8 %collective-permute-start = (f32[12,512]{1,0:T(8,128)S(1)}, f32[12,512]{1,0:T(8,128)S(1)}, u32[]{:S(2)}, u32[]{:S(2)}) collective-permute-start(f32[12,512]{1,0:T(8,128)S(1)} %slice.96), channel_id=1, source_target_pairs={{0,1},{1,2},{2,3},{4,5},{5,6},{6,7},{8,9},{9,10},{10,11},{12,13},{... | collective-permute-start | bytes 73736
  68.2 13.1 %collective-permute-start.3 = (f32[12,512]{1,0:T(8,128)S(1)}, f32[12,512]{1,0:T(8,128)S(1)}, u32[]{:S(2)}, u32[]{:S(2)}) collective-permute-start(f32[12,512]{1,0:T(8,128)S(1)} %slice.99), channel_id=1, source_target_pairs={{0,1},{1,2},{2,3},{4,5},{5,6},{6,7},{8,9},{9,10},{10,11},{12,13},{... | collective-permute-start | bytes 73736
  195.0 10.2 %collective-permute-start.5 = (f32[12,512]{1,0:T(8,128)S(1)}, f32[12,512]{1,0:T(8,128)S(1)}, u32[]{:S(2)}, u32[]{:S(2)}) collective-permute-start(f32[12,512]{1,0:T(8,128)S(1)} %slice.101), channel_id=1, source_target_pairs={{0,1},{1,2},{2,3},{4,5},{5,6},{6,7},{8,9},{9,10},{10,11},{12,13},{... | collective-permute-start | bytes 73736
  196.3 9.0 %collective-permute-start.6 = (f32[12,512]{1,0:T(8,128)S(1)}, f32[12,512]{1,0:T(8,128)S(1)}, u32[]{:S(2)}, u32[]{:S(2)}) collective-permute-start(f32[12,512]{1,0:T(8,128)S(1)} %slice.102), channel_id=1, source_target_pairs={{0,1},{1,2},{2,3},{4,5},{5,6},{6,7},{8,9},{9,10},{10,11},{12,13},{... | collective-permute-start | bytes 73736
  200.3 5.2 %collective-permute-start.4 = (f32[12,512]{1,0:T(8,128)S(1)}, f32[12,512]{1,0:T(8,128)S(1)}, u32[]{:S(2)}, u32[]{:S(2)}) collective-permute-start(f32[12,512]{1,0:T(8,128)S(1)} %slice.100), channel_id=1, source_target_pairs={{0,1},{1,2},{2,3},{4,5},{5,6},{6,7},{8,9},{9,10},{10,11},{12,13},{... | collective-permute-start | bytes 73736
  202.2 3.5 %collective-permute-start.7 = (f32[12,512]{1,0:T(8,128)S(1)}, f32[12,512]{1,0:T(8,128)S(1)}, u32[]{:S(2)}, u32[]{:S(2)}) collective-permute-start(f32[12,512]{1,0:T(8,128)S(1)} %slice.103), channel_id=1, source_target_pairs={{0,1},{1,2},{2,3},{4,5},{5,6},{6,7},{8,9},{9,10},{10,11},{12,13},{... | collective-permute-start | bytes 73736
  206.1 14.5 %slice-start = ((s8[14680064]{0:T(1024)(128)(4,1)}), s8[2097152]{0:T(1024)(128)(4,1)S(1)}, s32[]{:S(2)}) async-start(s8[14680064]{0:T(1024)(128)(4,1)} %bitcast.144), calls=%async_computation.1 | async-start | bytes 4194304
  206.5 14.2 %slice-start.1 = ((s8[14680064]{0:T(1024)(128)(4,1)}), s8[4194304]{0:T(1024)(128)(4,1)S(1)}, s32[]{:S(2)}) async-start(s8[14680064]{0:T(1024)(128)(4,1)} %bitcast.144), calls=%async_computation.2 | async-start | bytes 8388608
  206.5 14.2 %slice-start.2 = ((s8[14680064]{0:T(1024)(128)(4,1)}), s8[4194304]{0:T(1024)(128)(4,1)S(1)}, s32[]{:S(2)}) async-start(s8[14680064]{0:T(1024)(128)(4,1)} %bitcast.144), calls=%async_computation.3 | async-start | bytes 8388608
  206.5 14.2 %slice-start.3 = ((s8[14680064]{0:T(1024)(128)(4,1)}), s8[4194304]{0:T(1024)(128)(4,1)S(1)}, s32[]{:S(2)}) async-start(s8[14680064]{0:T(1024)(128)(4,1)} %bitcast.144), calls=%async_computation.4 | async-start | bytes 8388608
  258.7 15.5 %collective-permute-start.8 = (bf16[14,1024]{1,0:T(8,128)(2,1)S(1)}, bf16[14,1024]{1,0:T(8,128)(2,1)S(1)}, u32[]{:S(2)}, u32[]{:S(2)}) collective-permute-start(bf16[14,1024]{1,0:T(8,128)(2,1)S(1)} %slice.104), channel_id=1, source_target_pairs={{0,4},{4,8},{8,12},{12,16},{16,20},{20,24},{24,28},{1,5},{5,9},{9,... | collective-permute-start | bytes 86024
Sparse Core Ops, SparseCore 0:
  98.4 67.2 all-gather.5
